TPU v7x, 32 devices: a whole 2x2x4 slice. The times are simulated.
32 devices in a mesh: rep: 2 (over x), fs: 8 (over z, y), tp: 2 (over core).
Axes of the slice: x: 2, y: 2, z: 4, core: 2. Of those that a mesh axis runs over, the one named last changes fastest.
Arguments:
- tokens: bfloat16 [8192, 2048], P(('rep', 'fs')), may hold values from -3 to 3
- mixer_gain: float32 [2048], replicated, may hold values from 0.1 to 1.9
- mix_weight: bfloat16 [2048, 1024], P('fs', 'tp'), may hold values from -0.125 to 0.125
- mixer_conv: float32 [4, 1024], P(None, 'tp'), may hold values from -3 to 3
- mixer_offset: float32 [1024], P('tp'), may hold values from -0.06 to 0.06
- recur_weight: bfloat16 [8, 128, 128], P('tp'), may hold values from -0.5 to 0.5
- recur_bias: float32 [1024], P('tp'), may hold values from -3 to 3
- input_weight: bfloat16 [8, 128, 128], P('tp'), may hold values from -0.5 to 0.5
- input_bias: float32 [1024], P('tp'), may hold values from 1 to 3
- decay_logit: float32 [1024], P('tp'), may hold values from 4 to 11
- out_weight: bfloat16 [1024, 2048], P('tp', 'fs'), may hold values from -0.375 to 0.375
- channel_gain: float32 [2048], replicated, may hold values from 0.1 to 1.9
- gate_weight: bfloat16 [2048, 6144], P('fs', 'tp'), may hold values from -0.125 to 0.125
- up_weight: bfloat16 [2048, 6144], P('fs', 'tp'), may hold values from -0.125 to 0.125
- gate_conv: float32 [3, 6144], P(None, 'tp'), may hold values from -3.5 to 3.5
- gate_offset: float32 [6144], P('tp'), may hold values from -3 to 3
- down_weight: bfloat16 [6144, 2048], P('tp', 'fs'), may hold values from -0.078125 to 0.078125
Outputs:
- layer_out: bfloat16 [8192, 2048], P(('rep', 'fs'))
All inputs are finite; a program needn't handle non-finite values.
Results may differ from a plain program's by a relative error of at most 0.023.
Values may be sent and summed in bfloat16 or wider, within the bound.
A program may use at most 128 MiB of HBM per device.

v0:
```python
import jax
import jax.numpy as jnp
from jax import lax
from jax.sharding import PartitionSpec as P

epsilon = 1e-06
lru_scale = 8.0


def rms_rows(values, gain_row):
    widened = values.astype(jnp.float32)
    scaled = widened * lax.rsqrt(jnp.mean(widened * widened, axis=-1, keepdims=True) + epsilon)
    return (scaled * gain_row).astype(jnp.bfloat16)


def causal_conv(values, tap_rows, offset):
    width = tap_rows.shape[0]
    length = values.shape[-2]
    padding = [(0, 0)] * (values.ndim - 2) + [(width - 1, 0), (0, 0)]
    padded = jnp.pad(values, padding)
    total = offset + padded[..., 0:length, :] * tap_rows[0]
    for tap_index in range(1, width):
        total = total + padded[..., tap_index : tap_index + length, :] * tap_rows[tap_index]
    return total


def linear_combine(earlier, latter):
    decay_early, sum_early = earlier
    decay_late, sum_late = latter
    return (decay_early * decay_late, decay_late * sum_early + sum_late)


def block_gate(blocked, weight, bias):
    length = blocked.shape[0]
    product = jnp.einsum("lhi,hij->lhj", blocked, weight, preferred_element_type=jnp.float32)
    return jax.nn.sigmoid(product.reshape(length, bias.shape[0]) + bias)


def local(
    tokens,
    mixer_gain,
    mix_weight,
    mixer_conv,
    mixer_offset,
    recur_weight,
    recur_bias,
    input_weight,
    input_bias,
    decay_logit,
    out_weight,
    channel_gain,
    gate_weight,
    up_weight,
    gate_conv,
    gate_offset,
    down_weight,
):
    normed = rms_rows(tokens, mixer_gain)
    mixer_full = lax.all_gather(mix_weight, "fs", axis=0, tiled=True)
    branch = jnp.dot(normed, mixer_full, preferred_element_type=jnp.float32).astype(jnp.bfloat16)
    smoothed = causal_conv(branch.astype(jnp.float32), mixer_conv, mixer_offset).astype(
        jnp.bfloat16
    )
    length = smoothed.shape[0]
    blocked = smoothed.reshape(length, recur_weight.shape[0], recur_weight.shape[1])
    recur_gate = block_gate(blocked, recur_weight, recur_bias)
    input_gate = block_gate(blocked, input_weight, input_bias)
    log_decay = lru_scale * recur_gate * jax.nn.log_sigmoid(decay_logit)
    drive = jnp.sqrt(-jnp.expm1(2.0 * log_decay)) * (input_gate * smoothed.astype(jnp.float32))
    _, states = lax.associative_scan(linear_combine, (jnp.exp(log_decay), drive), axis=0)
    recurrent = states.astype(jnp.bfloat16)
    out_full = lax.all_gather(out_weight, "fs", axis=1, tiled=True)
    mixer_term = jnp.dot(recurrent, out_full, preferred_element_type=jnp.float32)
    mixer_sum = lax.psum(mixer_term.astype(jnp.bfloat16), "tp").astype(jnp.float32)
    residual = (tokens.astype(jnp.float32) + mixer_sum).astype(jnp.bfloat16)
    normed_mlp = rms_rows(residual, channel_gain)
    gate_total = jnp.dot(
        normed_mlp,
        lax.all_gather(gate_weight, "fs", axis=0, tiled=True),
        preferred_element_type=jnp.float32,
    )
    up_total = jnp.dot(
        normed_mlp,
        lax.all_gather(up_weight, "fs", axis=0, tiled=True),
        preferred_element_type=jnp.float32,
    )
    gate_rows = gate_total.astype(jnp.bfloat16)
    up_rows = up_total.astype(jnp.bfloat16)
    gate_mixed = causal_conv(gate_rows.astype(jnp.float32), gate_conv, gate_offset)
    hidden = (jax.nn.gelu(gate_mixed) * up_rows.astype(jnp.float32)).astype(jnp.bfloat16)
    terms = jnp.dot(
        hidden,
        lax.all_gather(down_weight, "fs", axis=1, tiled=True),
        preferred_element_type=jnp.float32,
    )
    mlp_sum = lax.psum(terms.astype(jnp.bfloat16), "tp").astype(jnp.float32)
    return (residual.astype(jnp.float32) + mlp_sum).astype(jnp.bfloat16)


def solution(mesh):
    in_specs = (
        P(("rep", "fs"), None),
        P(),
        P("fs", "tp"),
        P(None, "tp"),
        P("tp"),
        P("tp", None, None),
        P("tp"),
        P("tp", None, None),
        P("tp"),
        P("tp"),
        P("tp", "fs"),
        P(),
        P("fs", "tp"),
        P("fs", "tp"),
        P(None, "tp"),
        P("tp"),
        P("tp", "fs"),
    )
    out_specs = P(("rep", "fs"), None)
    return jax.shard_map(local, mesh=mesh, in_specs=in_specs, out_specs=out_specs, check_vma=False)
```

profile of v0, /device:TPU:0, one launch (start us, length us, event | category | flops | bytes accessed | tf_op | source)
XLA Modules:
  0.0 773.1 jit_solution(14933840304383471797)
XLA Ops:
  8.9 2.1 fusion.10
  11.7 49.6 %all-gather.6.cloned.1.call-done = bf16[2048,512]{1,0:T(8,128)(2,1)} async-done(((bf16[256,512]{1,0:T(8,128)(2,1)}), bf16[2048,512]{1,0:T(8,128)(2,1)}) %all-gather.6.cloned.1.call-update) | async-done | bytes 2097168 | tf_op jit(solution)/shard_map/all_gather | solution.py:59
  61.3 3.5 fusion.30
  68.8 3.2 fusion.47
  72.0 2.1 slice.255
  74.0 2.1 slice.256
  76.1 2.1 slice.254
  78.1 2.1 slice.258
  80.2 1.7 fusion.63
  87.4 2.0 fusion.64
  90.8 1.6 slice.266
  92.4 1.6 slice.270
  94.0 1.8 fusion.65
  97.0 1.5 slice.272
  98.6 1.5 slice.276
  100.1 1.6 fusion.66
  104.6 1.4 slice.278
  132.0 1.5 slice.277
  133.5 1.4 slice.310
  136.2 1.5 slice.271
  139.0 1.6 slice.265
  156.0 2.7 pad.81
  159.2 4.5 convolution_convert_fusion.2
  165.7 18.0 %all-reduce.23.cloned.1.call-done = bf16[512,2048]{1,0:T(8,128)(2,1)} async-done(((bf16[512,2048]{1,0:T(8,128)(2,1)}), bf16[512,2048]{1,0:T(8,128)(2,1)}) %all-reduce.23.cloned.1.call-update) | async-done | bytes 2097168 | tf_op jit(solution)/shard_map/psum | solution.py:74
  183.7 3.2 fusion.14
  186.9 176.1 %all-gather.10.cloned.1.call-done = bf16[2048,3072]{1,0:T(8,128)(2,1)} async-done(((bf16[256,3072]{1,0:T(8,128)(2,1)}), bf16[2048,3072]{1,0:T(8,128)(2,1)}) %all-gather.10.cloned.1.call-update) | async-done | bytes 12582928 | tf_op jit(solution)/shard_map/all_gather | solution.py:79
  363.0 11.4 %fusion.9 = f32[512,3072]{1,0:T(8,128)} fusion(bf16[2048,3072]{1,0:T(8,128)(2,1)} %all-gather.10.cloned.1.call-done, bf16[512,2048]{1,0:T(8,128)(2,1)S(1)} %get-tuple-element.6, f32[2048]{0:T(1024)S(1)} %copy-done.10, f32[512]{0:T(512)S(1)} %add_rsqrt_fusion), kind=kOutput, calls=%fused_computation.18 | convolution fusion | flops 6449790976 | bytes 20981760 | tf_op jit(solution)/shard_map/dot_general | solution.py:77
  374.5 164.9 %all-gather.12.cloned.1.call-done = bf16[2048,3072]{1,0:T(8,128)(2,1)} async-done(((bf16[256,3072]{1,0:T(8,128)(2,1)}), bf16[2048,3072]{1,0:T(8,128)(2,1)}) %all-gather.12.cloned.1.call-update) | async-done | bytes 12582928 | tf_op jit(solution)/shard_map/all_gather | solution.py:84
  539.4 176.2 %all-gather.14.cloned.1.call-done = bf16[3072,2048]{1,0:T(8,128)(2,1)} async-done(((bf16[3072,256]{1,0:T(8,128)(2,1)}), bf16[3072,2048]{1,0:T(8,128)(2,1)}) %all-gather.14.cloned.1.call-update) | async-done | bytes 12582928 | tf_op jit(solution)/shard_map/all_gather | solution.py:93
  715.6 27.3 %fusion.20 = bf16[512,2048]{1,0:T(8,128)(2,1)} fusion(bf16[3072,2048]{1,0:T(8,128)(2,1)} %all-gather.14.cloned.1.call-done, f32[512,3072]{1,0:T(8,128)} %fusion.9, f32[3072]{0:T(1024)S(1)} %bitcast.38, f32[3072]{0:T(1024)S(1)} %bitcast.39, f32[3072]{0:T(1024)S(1)} %bitcast.37, f32[3072]{0:T(1024)S(1)} %copy-done.9, ...), kind=kOutput, calls=%fused_computation.28 | convolution fusion | flops 12918456320 | bytes 35710976 | tf_op jit(solution)/shard_map/dot_general | solution.py:91
  743.0 19.6 %all-reduce.25.cloned.1.call-done = bf16[512,2048]{1,0:T(8,128)(2,1)} async-done(((bf16[512,2048]{1,0:T(8,128)(2,1)}), bf16[512,2048]{1,0:T(8,128)(2,1)}) %all-reduce.25.cloned.1.call-update) | async-done | bytes 2097168 | tf_op jit(solution)/shard_map/psum | solution.py:96
  762.6 3.7 fusion.17
  (131 shorter events, 64.0 us)
Async XLA Ops:
  6.5 58.8 %copy-start = (bf16[4,128,128]{2,1,0:T(8,128)(2,1)S(1)}, bf16[4,128,128]{2,1,0:T(8,128)(2,1)}, u32[]{:S(2)}) copy-start(bf16[4,128,128]{2,1,0:T(8,128)(2,1)} %param.22) | copy-start | bytes 393220
  6.5 54.8 %all-gather.6.cloned.1.call-start = ((), (), s32[]{:S(2)}) async-start(), calls=%async_computation | async-start | bytes 2359296 | tf_op jit(solution)/shard_map/all_gather | solution.py:59
  7.3 151.9 %all-gather.8.cloned.1.call-start = ((), (), s32[]{:S(2)}) async-start(), calls=%async_computation.1 | async-start | bytes 2359296 | tf_op jit(solution)/shard_map/all_gather | solution.py:72
  8.0 175.7 %all-reduce.23.cloned.1.call-start = ((), (), s32[]{:S(2)}) async-start(), calls=%async_computation.2 | async-start | bytes 4194304 | tf_op jit(solution)/shard_map/psum | solution.py:74
  11.0 53.9 %copy-start.5 = (f32[512]{0:T(512)S(1)}, f32[512]{0:T(512)}, u32[]{:S(2)}) copy-start(f32[512]{0:T(512)} %param.21) | copy-start | bytes 6148
  64.8 2.2 copy-start.3
  65.4 3.4 copy-start.7
  65.4 3.4 copy-start.8
  145.4 10.2 %copy-start.2 = (f32[127,512]{1,0:T(8,128)S(1)}, f32[127,512]{1,0:T(8,128)}, u32[]{:S(2)}) copy-start(f32[127,512]{1,0:T(8,128)} %slice.316) | copy-start | bytes 780292
  145.4 10.3 %copy-start.6 = (f32[1,512]{1,0:T(1,128)S(1)}, f32[1,512]{1,0:T(1,128)}, u32[]{:S(2)}) copy-start(f32[1,512]{1,0:T(1,128)} %slice.325) | copy-start | bytes 6148
  163.7 2.0 copy-start.4
  163.7 199.3 %all-gather.10.cloned.1.call-start = ((), (), s32[]{:S(2)}) async-start(), calls=%async_computation.3 | async-start | bytes 14155776 | tf_op jit(solution)/shard_map/all_gather | solution.py:79
  164.3 375.1 %all-gather.12.cloned.1.call-start = ((), (), s32[]{:S(2)}) async-start(), calls=%async_computation.4 | async-start | bytes 14155776 | tf_op jit(solution)/shard_map/all_gather | solution.py:84
  164.9 198.2 %copy-start.10 = (f32[2048]{0:T(1024)S(1)}, f32[2048]{0:T(1024)}, u32[]{:S(2)}) copy-start(f32[2048]{0:T(1024)} %param.28) | copy-start | bytes 24580
  164.9 550.7 %all-gather.14.cloned.1.call-start = ((), (), s32[]{:S(2)}) async-start(), calls=%async_computation.5 | async-start | bytes 14155776 | tf_op jit(solution)/shard_map/all_gather | solution.py:93
  165.4 597.1 %all-reduce.25.cloned.1.call-start = ((), (), s32[]{:S(2)}) async-start(), calls=%async_computation.6 | async-start | bytes 4194304 | tf_op jit(solution)/shard_map/psum | solution.py:96
  363.0 352.6 %copy-start.9 = (f32[3072]{0:T(1024)S(1)}, f32[3072]{0:T(1024)}, u32[]{:S(2)}) copy-start(f32[3072]{0:T(1024)} %param.32) | copy-start | bytes 36868
  743.0 23.3 %copy-start.1 = (bf16[4,128,128]{2,1,0:T(8,128)(2,1)S(1)}, bf16[4,128,128]{2,1,0:T(8,128)(2,1)}, u32[]{:S(2)}) copy-start(bf16[4,128,128]{2,1,0:T(8,128)(2,1)} %param.22) | copy-start | bytes 393220
Sparse Core Ops, SparseCore 0:
  9.5 51.7 all-gather.5
  63.3 48.8 all-gather.7
  163.8 19.8 all-reduce.22
  185.7 177.2 all-gather.9
  365.1 174.2 all-gather.11
  541.3 174.2 all-gather.13
  743.1 19.4 all-reduce.24
where the time goes:
time: 775 us; the launch traced here: 773 us
  waiting for transfers between devices  607 us (78%)
  local copies, waits for them, and re-layouts  68.9 us (9%)
  matrix products  47.5 us (6%)
  other arithmetic  34.9 us (5%)
  between operations  13.9 us (2%)
    all_gather x1, waiting for transfers between devices, local(): lax.all_gather(down_weight, 'fs', axis=1, tiled=True)  176 us
    all_gather x1, waiting for transfers between devices, local(): lax.all_gather(gate_weight, 'fs', axis=0, tiled=True)  176 us
    all_gather x1, waiting for transfers between devices, local(): lax.all_gather(up_weight, 'fs', axis=0, tiled=True)  165 us
    slice x53, local copies, waits for them, and re-layouts, local(): lax.associative_scan(linear_combine, (jnp.exp(log_decay), drive), axis=0)  62.1 us
    all_gather x1, waiting for transfers between devices, local(): mixer_full = lax.all_gather(mix_weight, 'fs', axis=0, tiled=True)  49.6 us
    dot_general x1, matrix products, local(): jnp.dot(hidden, lax.all_gather(down_weight, 'fs', axis=1, tiled=True), pr...  27.3 us
    psum x1, waiting for transfers between devices, local(): mlp_sum = lax.psum(terms.astype(jnp.bfloat16), 'tp').astype(jnp.float32)  19.6 us
    psum x1, waiting for transfers between devices, local(): lax.psum(mixer_term.astype(jnp.bfloat16), 'tp').astype(jnp.float32)  18 us
  transfers between devices with their start and end apart: 7, of which 6 were waited for; matrix products, arithmetic and copies ran while one was open for 15% of the time, Pallas kernels for 0%

commit v1 on v0

v1 whole, which is shorter than its diff:
```python
import functools

import jax
import jax.numpy as jnp
from jax import lax
from jax.experimental import pallas as pl
from jax.experimental.pallas import tpu as pltpu
from jax.sharding import PartitionSpec as P

epsilon = 1e-06
lru_scale = 8.0


def rms_rows(values, gain_row):
    widened = values.astype(jnp.float32)
    scaled = widened * lax.rsqrt(jnp.mean(widened * widened, axis=-1, keepdims=True) + epsilon)
    return (scaled * gain_row).astype(jnp.bfloat16)


def causal_conv(values, tap_rows, offset):
    width = tap_rows.shape[0]
    length = values.shape[-2]
    padding = [(0, 0)] * (values.ndim - 2) + [(width - 1, 0), (0, 0)]
    padded = jnp.pad(values, padding)
    total = offset + padded[..., 0:length, :] * tap_rows[0]
    for tap_index in range(1, width):
        total = total + padded[..., tap_index : tap_index + length, :] * tap_rows[tap_index]
    return total


def one_minus_exp(v):
    series = 1.0 + v * (1.0 / 7.0)
    for order in (6.0, 5.0, 4.0, 3.0, 2.0):
        series = 1.0 + v * (1.0 / order) * series
    return jnp.where(v > -0.25, -v * series, 1.0 - jnp.exp(v))


def mixer_kernel(
    branch_ref, taps_ref, offset_ref, recur_ref, recur_bias_ref, input_ref, input_bias_ref, rate_ref, out_ref
):
    branch = branch_ref[...].astype(jnp.float32)
    length = branch.shape[0]
    width = taps_ref.shape[0]
    rows = lax.broadcasted_iota(jnp.int32, branch.shape, 0)

    def shifted(values, step, fill):
        return jnp.where(rows >= step, pltpu.roll(values, step, 0), fill)

    total = offset_ref[...] + branch * taps_ref[width - 1 : width, :]
    for back in range(1, width):
        total = total + shifted(branch, back, 0.0) * taps_ref[width - 1 - back : width - back, :]
    smoothed = total.astype(jnp.bfloat16)
    recur = jnp.dot(smoothed, recur_ref[0], preferred_element_type=jnp.float32)
    recur_gate = jax.nn.sigmoid(recur + recur_bias_ref[...])
    gated = jnp.dot(smoothed, input_ref[0], preferred_element_type=jnp.float32)
    input_gate = jax.nn.sigmoid(gated + input_bias_ref[...])
    log_decay = recur_gate * rate_ref[...]
    state = jnp.sqrt(one_minus_exp(2.0 * log_decay)) * (input_gate * smoothed.astype(jnp.float32))
    decay = jnp.exp(log_decay)
    step = 1
    while step < length:
        state = state + decay * shifted(state, step, 0.0)
        if 2 * step < length:
            decay = decay * shifted(decay, step, 1.0)
        step *= 2
    out_ref[...] = state.astype(jnp.bfloat16)


def mixer(branch, taps, offset, recur_weight, recur_bias, input_weight, input_bias, rate):
    length, channels = branch.shape
    blocks, dim, _ = recur_weight.shape
    column = lambda rows: pl.BlockSpec((rows, dim), lambda k: (0, k))
    square = pl.BlockSpec((1, dim, dim), lambda k: (k, 0, 0))
    row = lambda v: v.reshape(1, channels)
    return pl.pallas_call(
        mixer_kernel,
        name="mixer",
        grid=(blocks,),
        in_specs=[
            column(length),
            column(taps.shape[0]),
            column(1),
            square,
            column(1),
            square,
            column(1),
            column(1),
        ],
        out_specs=column(length),
        out_shape=jax.ShapeDtypeStruct((length, channels), jnp.bfloat16),
        cost_estimate=pl.CostEstimate(
            flops=60 * length * channels + 4 * length * channels * dim,
            bytes_accessed=4 * length * channels,
            transcendentals=5 * length * channels,
        ),
    )(
        branch,
        taps,
        row(offset),
        recur_weight,
        row(recur_bias),
        input_weight,
        row(input_bias),
        row(rate),
    )


def shift(values, axis, count, step):
    return lax.ppermute(values, axis, [(i, (i + step) % count) for i in range(count)])


def take(values, index, size, axis=0):
    return lax.dynamic_slice_in_dim(values, index * size, size, axis)


def scatter_rows(partial, n_tp, me):
    size = partial.shape[0] // n_tp
    total = take(partial, me, size).astype(jnp.float32)
    for step in range(1, n_tp):
        sent = take(partial, lax.rem(me + step, n_tp), size)
        total = total + shift(sent, "tp", n_tp, step).astype(jnp.float32)
    return total


def collect_rows(share, n_tp, me):
    size = share.shape[0]
    if n_tp == 2:
        other = shift(share, "tp", n_tp, 1)
        first = jnp.where(me == 0, share, other)
        second = jnp.where(me == 0, other, share)
        return jnp.concatenate([first, second], axis=0)
    whole = jnp.zeros((size * n_tp, share.shape[1]), share.dtype)
    whole = lax.dynamic_update_slice_in_dim(whole, share, me * size, 0)
    for step in range(1, n_tp):
        got = shift(share, "tp", n_tp, step)
        whole = lax.dynamic_update_slice_in_dim(whole, got, lax.rem(me - step + n_tp, n_tp) * size, 0)
    return whole


def local(
    n_rep,
    n_tp,
    tokens,
    mixer_gain,
    mix_weight,
    mixer_conv,
    mixer_offset,
    recur_weight,
    recur_bias,
    input_weight,
    input_bias,
    decay_logit,
    out_weight,
    channel_gain,
    gate_weight,
    up_weight,
    gate_conv,
    gate_offset,
    down_weight,
):
    rep = lax.axis_index("rep")
    tp = lax.axis_index("tp")
    length = tokens.shape[0]
    units = gate_weight.shape[1] // n_rep

    mixer_full = lax.all_gather(mix_weight, "fs", axis=0, tiled=True)
    out_full = lax.all_gather(out_weight, "fs", axis=1, tiled=True)
    gate_full = lax.all_gather(take(gate_weight, rep, units, 1), "fs", axis=0, tiled=True)
    up_full = lax.all_gather(take(up_weight, rep, units, 1), "fs", axis=0, tiled=True)
    down_full = lax.all_gather(take(down_weight, rep, units, 0), "fs", axis=1, tiled=True)
    gate_taps = take(gate_conv, rep, units, 1)
    gate_base = take(gate_offset, rep, units, 0)

    normed = rms_rows(tokens, mixer_gain)
    branch = jnp.dot(normed, mixer_full, preferred_element_type=jnp.float32).astype(jnp.bfloat16)
    recurrent = mixer(
        branch,
        mixer_conv,
        mixer_offset,
        recur_weight,
        recur_bias,
        input_weight,
        input_bias,
        lru_scale * jax.nn.log_sigmoid(decay_logit),
    )
    mixer_term = jnp.dot(recurrent, out_full, preferred_element_type=jnp.float32)
    mixer_share = scatter_rows(mixer_term.astype(jnp.bfloat16), n_tp, tp)
    rows = length // n_tp
    residual = (take(tokens, tp, rows).astype(jnp.float32) + mixer_share).astype(jnp.bfloat16)
    normed_share = rms_rows(residual, channel_gain)

    shares = [normed_share]
    for step in range(1, n_rep):
        shares.append(shift(normed_share, "rep", n_rep, step))

    def channel_mixer(share):
        rows_in = collect_rows(share, n_tp, tp)
        gate_rows = jnp.dot(rows_in, gate_full, preferred_element_type=jnp.float32)
        up_rows = jnp.dot(rows_in, up_full, preferred_element_type=jnp.float32)
        gate_rows = gate_rows.astype(jnp.bfloat16)
        up_rows = up_rows.astype(jnp.bfloat16)
        gate_mixed = causal_conv(gate_rows.astype(jnp.float32), gate_taps, gate_base)
        hidden = (jax.nn.gelu(gate_mixed) * up_rows.astype(jnp.float32)).astype(jnp.bfloat16)
        return jnp.dot(hidden, down_full, preferred_element_type=jnp.float32).astype(jnp.bfloat16)

    own_terms = channel_mixer(shares[0])
    total = None
    for step in range(1, n_rep):
        summed = scatter_rows(channel_mixer(shares[step]), n_tp, tp).astype(jnp.bfloat16)
        back = shift(summed, "rep", n_rep, -step).astype(jnp.float32)
        total = back if total is None else total + back
    own = scatter_rows(own_terms, n_tp, tp)
    total = own if total is None else own + total
    result = (residual.astype(jnp.float32) + total).astype(jnp.bfloat16)
    return collect_rows(result, n_tp, tp)


def solution(mesh):
    in_specs = (
        P(("rep", "fs"), None),
        P(),
        P("fs", "tp"),
        P(None, "tp"),
        P("tp"),
        P("tp", None, None),
        P("tp"),
        P("tp", None, None),
        P("tp"),
        P("tp"),
        P("tp", "fs"),
        P(),
        P("fs", "tp"),
        P("fs", "tp"),
        P(None, "tp"),
        P("tp"),
        P("tp", "fs"),
    )
    out_specs = P(("rep", "fs"), None)
    body = functools.partial(local, mesh.shape["rep"], mesh.shape["tp"])
    return jax.shard_map(body, mesh=mesh, in_specs=in_specs, out_specs=out_specs, check_vma=False)
```

time: 775 us -> 494 us (0.64)
  waiting for transfers between devices: 607 us -> 388 us
  local copies, waits for them, and re-layouts: 68.9 us -> 10.2 us
  other arithmetic: 34.9 us -> 13.5 us
  matrix products: 47.5 us -> 58.3 us
    all_gather x3, waiting for transfers between devices: 517 us -> 246 us  [the longest x1 99.6 us: local(): lax.all_gather(take(down_weight, rep, units, 0), 'fs', axis=1, tiled=True)]
    slice x53 -> x0, local copies, waits for them, and re-layouts: 62.1 us -> none  [local(): lax.associative_scan(linear_combine, (jnp.exp(log_decay), drive), axis=0)]
    ppermute x0 -> x8, waiting for transfers between devices: none -> 52.9 us  [shift(): lax.ppermute(values, axis, [(i, (i + step) % count) for i in range(count)])]
    all_gather x1, waiting for transfers between devices: 0.02 us -> 41.6 us  [local(): out_full = lax.all_gather(out_weight, 'fs', axis=1, tiled=True)]
    psum x2 -> x0, waiting for transfers between devices: 37.6 us -> none  [the longest x1 19.6 us: local(): mlp_sum = lax.psum(terms.astype(jnp.bfloat16), 'tp').astype(jnp.float32)]
    mul x8 -> x1, other arithmetic: 11.9 us -> 0.61 us  [local(): lru_scale * jax.nn.log_sigmoid(decay_logit)]
    dot_general x4, matrix products: 39.5 us -> 50.3 us  [the longest x2 33 us: channel_mixer(): jnp.dot(hidden, down_full, preferred_element_type=jnp.float32)]
    dynamic_slice x0 -> x7, local copies, waits for them, and re-layouts: none -> 9.25 us  [take(): return lax.dynamic_slice_in_dim(values, index * size, size, axis)]
  transfers between devices with their start and end apart: 7 -> 13, of which waited for: 6 -> 9; matrix products, arithmetic and copies ran while one was open for 15% -> 13% of each run, Pallas kernels for 0% -> 1%
where the time goes in v1:
time: 494 us; the launch traced here: 493 us
  waiting for transfers between devices  388 us (79%)
  matrix products  58.3 us (12%)
  other arithmetic  13.5 us (3%)
  between operations  13.3 us (3%)
  local copies, waits for them, and re-layouts  10.2 us (2%)
  Pallas kernels  5.62 us (1%)
    all_gather x1, waiting for transfers between devices, local(): lax.all_gather(take(down_weight, rep, units, 0), 'fs', axis=1, tiled=True)  99.6 us
    all_gather x1, waiting for transfers between devices, local(): lax.all_gather(take(up_weight, rep, units, 1), 'fs', axis=0, tiled=True)  90.4 us
    all_gather x1, waiting for transfers between devices, local(): lax.all_gather(take(gate_weight, rep, units, 1), 'fs', axis=0, tiled=True)  55.7 us
    ppermute x8, waiting for transfers between devices, shift(): lax.ppermute(values, axis, [(i, (i + step) % count) for i in range(count)])  52.9 us
    all_gather x1, waiting for transfers between devices, local(): mixer_full = lax.all_gather(mix_weight, 'fs', axis=0, tiled=True)  46.6 us
    all_gather x1, waiting for transfers between devices, local(): out_full = lax.all_gather(out_weight, 'fs', axis=1, tiled=True)  41.6 us
    dot_general x2, matrix products, channel_mixer(): jnp.dot(hidden, down_full, preferred_element_type=jnp.float32)  33 us
    dot_general x2, matrix products, channel_mixer(): gate_rows = jnp.dot(rows_in, gate_full, preferred_element_type=jnp.float32)  17.3 us
  transfers between devices with their start and end apart: 13, of which 9 were waited for; matrix products, arithmetic and copies ran while one was open for 13% of the time, Pallas kernels for 1%

profile of v1, /device:TPU:0, one launch (start us, length us, event | category | flops | bytes accessed | tf_op | source)
XLA Modules:
  0.0 493.3 jit_solution(5149734190778220731)
XLA Ops:
  8.1 1.0 constant_dynamic-slice_fusion.4
  9.2 2.2 constant_dynamic-slice_fusion.3
  11.4 2.1 constant_dynamic-slice_fusion.2
  14.7 46.6 %all-gather.6.cloned.1.call-done = bf16[2048,512]{1,0:T(8,128)(2,1)} async-done(((bf16[256,512]{1,0:T(8,128)(2,1)}), bf16[2048,512]{1,0:T(8,128)(2,1)}) %all-gather.6.cloned.1.call-update) | async-done | bytes 2097168 | tf_op jit(solution)/shard_map/all_gather | solution.py:166
  61.3 3.7 fusion.31.branch_ref
  65.0 5.6 %mixer.1 = bf16[512,512]{1,0:T(8,128)(2,1)} custom-call(bf16[512,512]{1,0:T(8,128)(2,1)} %fusion.31.branch_ref, f32[4,512]{1,0:T(4,128)} %taps_ref.1, f32[1,512]{1,0:T(1,128)} %bitcast.14, bf16[4,128,128]{2,1,0:T(8,128)(2,1)} %recur_ref.1, f32[1,512]{1,0:T(1,128)} %bitcast.15, bf16[4,128,128]{2,1,0:T(8,128)(2,1)} %input_ref.1, f32[1,512]{1,0:T(1,128)} %bitcast.16, ...), custom_call_target="tpu_custom_call" | custom-call | flops 149946368 | bytes 1048576 | tf_op jit(solution)/shard_map/mixer/pallas_call | solution.py:75
  70.6 41.6 %all-gather.8.cloned.1.call-done = bf16[512,2048]{1,0:T(8,128)(2,1)} async-done(((bf16[512,256]{1,0:T(8,128)(2,1)}), bf16[512,2048]{1,0:T(8,128)(2,1)}) %all-gather.8.cloned.1.call-update) | async-done | bytes 2097168 | tf_op jit(solution)/shard_map/all_gather | solution.py:167
  112.2 4.3 convolution_convert_fusion.6
  116.6 1.3 constant_dynamic-slice_fusion.5
  118.0 2.8 collective-permute-done
  120.8 2.3 fusion.23
  123.1 1.3 fusion.25
  124.3 1.5 collective-permute-start.3
  125.9 23.9 %collective-permute-done.3 = bf16[256,2048]{1,0:T(8,128)(2,1)S(1)} collective-permute-done((bf16[256,2048]{1,0:T(8,128)(2,1)}, bf16[256,2048]{1,0:T(8,128)(2,1)S(1)}, u32[]{:S(2)}, u32[]{:S(2)}) %collective-permute-start.3) | collective-permute-done | bytes 1048608 | tf_op jit(solution)/shard_map/ppermute | solution.py:109
  149.8 1.0 dynamic-slice_reduce_fusion.2
  150.8 3.3 broadcast_select_fusion.5
  154.1 1.5 broadcast_select_fusion.3
  155.6 55.7 %all-gather.10.cloned.1.call-done = bf16[2048,1536]{1,0:T(8,128)(2,1)} async-done(((bf16[256,1536]{1,0:T(8,128)(2,1)}), bf16[2048,1536]{1,0:T(8,128)(2,1)}) %all-gather.10.cloned.1.call-update) | async-done | bytes 6291472 | tf_op jit(solution)/shard_map/all_gather | solution.py:168
  211.3 8.5 %fusion.21 = f32[512,1536]{1,0:T(8,128)} fusion(bf16[2048,1536]{1,0:T(8,128)(2,1)} %all-gather.10.cloned.1.call-done, bf16[256,2048]{1,0:T(8,128)(2,1)} %get-tuple-element.15, bf16[256,2048]{1,0:T(8,128)(2,1)} %get-tuple-element.14), kind=kOutput, calls=%fused_computation.31 | convolution fusion | flops 3226992640 | bytes 11534336 | tf_op jit(solution)/shard_map/dot_general | solution.py:198
  219.9 90.4 %all-gather.12.cloned.1.call-done = bf16[2048,1536]{1,0:T(8,128)(2,1)} async-done(((bf16[256,1536]{1,0:T(8,128)(2,1)}), bf16[2048,1536]{1,0:T(8,128)(2,1)}) %all-gather.12.cloned.1.call-update) | async-done | bytes 6291472 | tf_op jit(solution)/shard_map/all_gather | solution.py:169
  310.3 99.6 %all-gather.14.cloned.1.call-done = bf16[1536,2048]{1,0:T(8,128)(2,1)} async-done(((bf16[1536,256]{1,0:T(8,128)(2,1)}), bf16[1536,2048]{1,0:T(8,128)(2,1)}) %all-gather.14.cloned.1.call-update) | async-done | bytes 6291472 | tf_op jit(solution)/shard_map/all_gather | solution.py:170
  409.9 15.8 %convolution_convert_fusion = bf16[512,2048]{1,0:T(8,128)(2,1)S(1)} fusion(bf16[1536,2048]{1,0:T(8,128)(2,1)} %all-gather.14.cloned.1.call-done, f32[512,1536]{1,0:T(8,128)} %fusion.21, bf16[2048,1536]{1,0:T(8,128)(2,1)} %all-gather.12.cloned.1.call-done, f32[1536]{0:T(1024)S(1)} %get-tuple-element.7, f32[1536]{0:T(1024)S(1)} %get-tuple-element.6, ...), kind=kOutput, calls=%fused_computation.28 | convolution fusion | flops 6461849600 | bytes 19947520 | tf_op jit(solution)/shard_map/dot_general | solution.py:204
  425.7 1.1 constant_dynamic-slice_fusion
  426.8 8.8 %fusion.22 = f32[512,1536]{1,0:T(8,128)} fusion(bf16[2048,1536]{1,0:T(8,128)(2,1)} %all-gather.10.cloned.1.call-done, bf16[256,2048]{1,0:T(8,128)(2,1)} %get-tuple-element.13, bf16[256,2048]{1,0:T(8,128)(2,1)} %get-tuple-element.12), kind=kOutput, calls=%fused_computation.35 | convolution fusion | flops 3226992640 | bytes 11534336 | tf_op jit(solution)/shard_map/dot_general | solution.py:198
  435.6 17.2 %convolution_convert_fusion.3 = bf16[512,2048]{1,0:T(8,128)(2,1)} fusion(bf16[1536,2048]{1,0:T(8,128)(2,1)} %all-gather.14.cloned.1.call-done, f32[512,1536]{1,0:T(8,128)} %fusion.22, bf16[2048,1536]{1,0:T(8,128)(2,1)} %all-gather.12.cloned.1.call-done, f32[1536]{0:T(1024)S(1)} %get-tuple-element.7, f32[1536]{0:T(1024)S(1)} %get-tuple-element.6, ...), kind=kOutput, calls=%fused_computation.32 | convolution fusion | flops 6461849600 | bytes 19947520 | tf_op jit(solution)/shard_map/dot_general | solution.py:204
  452.7 1.4 constant_dynamic-slice_fusion.1
  454.8 1.6 add_convert_fusion
  456.4 1.6 collective-permute-start.6
  458.0 23.6 %collective-permute-done.6 = bf16[256,2048]{1,0:T(8,128)(2,1)S(1)} collective-permute-done((bf16[256,2048]{1,0:T(8,128)(2,1)S(1)}, bf16[256,2048]{1,0:T(8,128)(2,1)S(1)}, u32[]{:S(2)}, u32[]{:S(2)}) %collective-permute-start.6) | collective-permute-done | bytes 1048608 | tf_op jit(solution)/shard_map/ppermute | solution.py:109
  481.5 0.7 fusion.26
  482.4 2.6 collective-permute-done.7
  485.2 1.6 pad_maximum_fusion.2
  (42 shorter events, 3.7 us)
Async XLA Ops:
  6.5 1.5 copy-start
  6.5 54.8 %all-gather.6.cloned.1.call-start = ((), (), s32[]{:S(2)}) async-start(), calls=%async_computation | async-start | bytes 2359296 | tf_op jit(solution)/shard_map/all_gather | solution.py:166
  7.3 105.0 %all-gather.8.cloned.1.call-start = ((), (), s32[]{:S(2)}) async-start(), calls=%async_computation.1 | async-start | bytes 2359296 | tf_op jit(solution)/shard_map/all_gather | solution.py:167
  8.0 203.3 %all-gather.10.cloned.1.call-start = ((), (), s32[]{:S(2)}) async-start(), calls=%async_computation.2 | async-start | bytes 7077888 | tf_op jit(solution)/shard_map/all_gather | solution.py:168
  9.1 4.5 copy-start.2
  9.1 5.0 %copy-start.6 = (f32[512]{0:T(512)S(1)}, f32[512]{0:T(512)}, u32[]{:S(2)}) copy-start(f32[512]{0:T(512)} %param.26) | copy-start | bytes 6148
  9.1 52.2 %copy-start.7 = (f32[2048]{0:T(1024)S(1)}, f32[2048]{0:T(1024)}, u32[]{:S(2)}) copy-start(f32[2048]{0:T(1024)} %param.18) | copy-start | bytes 24580
  9.1 301.2 %all-gather.12.cloned.1.call-start = ((), (), s32[]{:S(2)}) async-start(), calls=%async_computation.3 | async-start | bytes 7077888 | tf_op jit(solution)/shard_map/all_gather | solution.py:169
  11.4 398.5 %all-gather.14.cloned.1.call-start = ((), (), s32[]{:S(2)}) async-start(), calls=%async_computation.4 | async-start | bytes 7077888 | tf_op jit(solution)/shard_map/all_gather | solution.py:170
  116.6 6.5 %copy-start.4 = (f32[2048]{0:T(1024)S(1)}, f32[2048]{0:T(1024)}, u32[]{:S(2)}) copy-start(f32[2048]{0:T(1024)} %param.28) | copy-start | bytes 24580
  117.9 2.9 collective-permute-start
  118.0 31.8 %copy-start.5 = (f32[3072]{0:T(1024)S(1)}, f32[3072]{0:T(1024)}, u32[]{:S(2)}) copy-start(f32[3072]{0:T(1024)} %param.32) | copy-start | bytes 36868
  124.3 25.4 %collective-permute-start.3 = (bf16[256,2048]{1,0:T(8,128)(2,1)}, bf16[256,2048]{1,0:T(8,128)(2,1)S(1)}, u32[]{:S(2)}, u32[]{:S(2)}) collective-permute-start(bf16[256,2048]{1,0:T(8,128)(2,1)} %fusion.25), channel_id=1, source_target_pairs={{0,16},{16,0},{1,17},{17,1},{2,18},{18,2},{3,19},{19,3},{4,20},{20... | collective-permute-start | bytes 3145736 | tf_op jit(solution)/shard_map/ppermute | solution.py:109
  125.8 24.9 %collective-permute-start.1 = (bf16[256,2048]{1,0:T(8,128)(2,1)}, bf16[256,2048]{1,0:T(8,128)(2,1)}, u32[]{:S(2)}, u32[]{:S(2)}) collective-permute-start(bf16[256,2048]{1,0:T(8,128)(2,1)} %fusion.25), channel_id=1, source_target_pairs={{0,1},{1,0},{2,3},{3,2},{4,5},{5,4},{6,7},{7,6},{8,9},{9,8},{10,11... | collective-permute-start | bytes 3145736 | tf_op jit(solution)/shard_map/ppermute | solution.py:109
  149.8 4.3 collective-permute-start.4
  426.8 28.0 %collective-permute-start.5 = (bf16[256,2048]{1,0:T(8,128)(2,1)}, bf16[256,2048]{1,0:T(8,128)(2,1)}, u32[]{:S(2)}, u32[]{:S(2)}) collective-permute-start(bf16[256,2048]{1,0:T(8,128)(2,1)} %constant_dynamic-slice_fusion), channel_id=1, source_target_pairs={{0,1},{1,0},{2,3},{3,2},{4,5},{5,4},{6,7},{7,6},{8,9},{9,8},{10,11... | collective-permute-start | bytes 3145736 | tf_op jit(solution)/shard_map/ppermute | solution.py:109
  452.7 28.8 %copy-start.3 = (bf16[512,2048]{1,0:T(8,128)(2,1)S(1)}, bf16[512,2048]{1,0:T(8,128)(2,1)}, u32[]{:S(2)}) copy-start(bf16[512,2048]{1,0:T(8,128)(2,1)} %convolution_convert_fusion.3) | copy-start | bytes 6291460
  454.2 3.8 collective-permute-start.2
  456.4 25.2 %collective-permute-start.6 = (bf16[256,2048]{1,0:T(8,128)(2,1)S(1)}, bf16[256,2048]{1,0:T(8,128)(2,1)S(1)}, u32[]{:S(2)}, u32[]{:S(2)}) collective-permute-start(bf16[256,2048]{1,0:T(8,128)(2,1)S(1)} %add_convert_fusion), channel_id=1, source_target_pairs={{0,16},{16,0},{1,17},{17,1},{2,18},{18,2},{3,19},{19,3},{4,20},{20... | collective-permute-start | bytes 3145736 | tf_op jit(solution)/shard_map/ppermute | solution.py:109
  482.3 2.7 collective-permute-start.7
  485.0 1.7 copy-start.1
Sparse Core Ops, SparseCore 0:
  9.5 51.7 all-gather.5
  63.3 48.8 all-gather.7
  114.4 96.8 all-gather.9
  213.4 96.8 all-gather.11
  312.2 97.6 all-gather.13

commit v2 on v1

--- a/solution.py
+++ b/solution.py
@@ -113,6 +113,22 @@
     return lax.dynamic_slice_in_dim(values, index * size, size, axis)
 
 
+def pair_gather(weight, count, axis):
+    groups = [list(range(parity, count, 2)) for parity in range(2)]
+    own = lax.all_gather(weight, "fs", axis=axis, axis_index_groups=groups, tiled=True)
+    other = lax.ppermute(own, "fs", [(i, i ^ 1) for i in range(count)])
+    return own, other
+
+
+def pair_columns(values, count, parity):
+    rows, width = values.shape
+    size = width // count
+    blocks = [values[:, i * size : (i + 1) * size] for i in range(count)]
+    even = jnp.concatenate(blocks[0::2], axis=1)
+    odd = jnp.concatenate(blocks[1::2], axis=1)
+    return jnp.where(parity == 0, even, odd), jnp.where(parity == 0, odd, even)
+
+
 def scatter_rows(partial, n_tp, me):
     size = partial.shape[0] // n_tp
     total = take(partial, me, size).astype(jnp.float32)
@@ -139,6 +155,7 @@
 
 def local(
     n_rep,
+    n_fs,
     n_tp,
     tokens,
     mixer_gain,
@@ -160,13 +177,16 @@
 ):
     rep = lax.axis_index("rep")
     tp = lax.axis_index("tp")
+    parity = lax.rem(lax.axis_index("fs"), 2)
     length = tokens.shape[0]
     units = gate_weight.shape[1] // n_rep
 
-    mixer_full = lax.all_gather(mix_weight, "fs", axis=0, tiled=True)
-    out_full = lax.all_gather(out_weight, "fs", axis=1, tiled=True)
-    gate_full = lax.all_gather(take(gate_weight, rep, units, 1), "fs", axis=0, tiled=True)
-    up_full = lax.all_gather(take(up_weight, rep, units, 1), "fs", axis=0, tiled=True)
+    both = jnp.concatenate([mix_weight, out_weight.T], axis=1)
+    both_full = lax.all_gather(both, "fs", axis=0, tiled=True)
+    channels = mix_weight.shape[1]
+    mixer_full, out_full = both_full[:, :channels], both_full[:, channels:]
+    gate_own, gate_other = pair_gather(take(gate_weight, rep, units, 1), n_fs, 0)
+    up_own, up_other = pair_gather(take(up_weight, rep, units, 1), n_fs, 0)
     down_full = lax.all_gather(take(down_weight, rep, units, 0), "fs", axis=1, tiled=True)
     gate_taps = take(gate_conv, rep, units, 1)
     gate_base = take(gate_offset, rep, units, 0)
@@ -183,7 +203,9 @@
         input_bias,
         lru_scale * jax.nn.log_sigmoid(decay_logit),
     )
-    mixer_term = jnp.dot(recurrent, out_full, preferred_element_type=jnp.float32)
+    mixer_term = lax.dot_general(
+        recurrent, out_full, (((1,), (1,)), ((), ())), preferred_element_type=jnp.float32
+    )
     mixer_share = scatter_rows(mixer_term.astype(jnp.bfloat16), n_tp, tp)
     rows = length // n_tp
     residual = (take(tokens, tp, rows).astype(jnp.float32) + mixer_share).astype(jnp.bfloat16)
@@ -195,8 +217,11 @@
 
     def channel_mixer(share):
         rows_in = collect_rows(share, n_tp, tp)
-        gate_rows = jnp.dot(rows_in, gate_full, preferred_element_type=jnp.float32)
-        up_rows = jnp.dot(rows_in, up_full, preferred_element_type=jnp.float32)
+        left, right = pair_columns(rows_in, n_fs, parity)
+        gate_rows = jnp.dot(left, gate_own, preferred_element_type=jnp.float32)
+        gate_rows = gate_rows + jnp.dot(right, gate_other, preferred_element_type=jnp.float32)
+        up_rows = jnp.dot(left, up_own, preferred_element_type=jnp.float32)
+        up_rows = up_rows + jnp.dot(right, up_other, preferred_element_type=jnp.float32)
         gate_rows = gate_rows.astype(jnp.bfloat16)
         up_rows = up_rows.astype(jnp.bfloat16)
         gate_mixed = causal_conv(gate_rows.astype(jnp.float32), gate_taps, gate_base)
@@ -236,5 +261,5 @@
         P("tp", "fs"),
     )
     out_specs = P(("rep", "fs"), None)
-    body = functools.partial(local, mesh.shape["rep"], mesh.shape["tp"])
+    body = functools.partial(local, mesh.shape["rep"], mesh.shape["fs"], mesh.shape["tp"])
     return jax.shard_map(body, mesh=mesh, in_specs=in_specs, out_specs=out_specs, check_vma=False)

time: 494 us -> 423 us (0.86)
  waiting for transfers between devices: 388 us -> 310 us
    ppermute x0 -> x2, waiting for transfers between devices: none -> 84 us  [pair_gather(): other = lax.ppermute(own, 'fs', [(i, i ^ 1) for i in range(count)])]
    all_gather x1, waiting for transfers between devices: 99.6 us -> 24.1 us  [local(): lax.all_gather(take(down_weight, rep, units, 0), 'fs', axis=1, tiled=True)]
    all_gather x4 -> x3, waiting for transfers between devices: 234 us -> 175 us  [the longest x2 104 us: pair_gather(): lax.all_gather(weight, 'fs', axis=axis, axis_index_groups=groups, tiled=T...]
    ppermute x8, waiting for transfers between devices: 52.9 us -> 26.4 us  [shift(): lax.ppermute(values, axis, [(i, (i + step) % count) for i in range(count)])]
    dot_general x3 -> x7, matrix products: 21.6 us -> 25.8 us  [the longest x2 10.9 us: channel_mixer(): jnp.dot(right, gate_other, preferred_element_type=jnp.float32)]
  transfers between devices with their start and end apart: 13 -> 14, of which waited for: 9 -> 7; matrix products, arithmetic and copies ran while one was open for 13% -> 15% of each run, Pallas kernels for 1% -> 1%
where the time goes in v2:
time: 423 us; the launch traced here: 422 us
  waiting for transfers between devices  310 us (73%)
  matrix products  60.3 us (14%)
  local copies, waits for them, and re-layouts  14 us (3%)
  between operations  13.5 us (3%)
  other arithmetic  11.9 us (3%)
  starting transfers between devices  6.79 us (2%)
  Pallas kernels  5.63 us (1%)
    all_gather x2, waiting for transfers between devices, pair_gather(): lax.all_gather(weight, 'fs', axis=axis, axis_index_groups=groups, tiled=T...  104 us
    ppermute x2, waiting for transfers between devices, pair_gather(): other = lax.ppermute(own, 'fs', [(i, i ^ 1) for i in range(count)])  84 us
    all_gather x1, waiting for transfers between devices, local(): both_full = lax.all_gather(both, 'fs', axis=0, tiled=True)  70.8 us
    dot_general x2, matrix products, channel_mixer(): jnp.dot(hidden, down_full, preferred_element_type=jnp.float32)  30.8 us
    ppermute x8, waiting for transfers between devices, shift(): lax.ppermute(values, axis, [(i, (i + step) % count) for i in range(count)])  26.4 us
    all_gather x1, waiting for transfers between devices, local(): lax.all_gather(take(down_weight, rep, units, 0), 'fs', axis=1, tiled=True)  24.1 us
    dot_general x2, matrix products, channel_mixer(): jnp.dot(right, gate_other, preferred_element_type=jnp.float32)  10.9 us
    dynamic_slice x7, local copies, waits for them, and re-layouts, take(): return lax.dynamic_slice_in_dim(values, index * size, size, axis)  9.03 us
  transfers between devices with their start and end apart: 14, of which 7 were waited for; matrix products, arithmetic and copies ran while one was open for 15% of the time, Pallas kernels for 1%

profile of v2, /device:TPU:0, one launch (start us, length us, event | category | flops | bytes accessed | tf_op | source)
XLA Modules:
  0.0 421.8 jit_solution(7286322764803237131)
XLA Ops:
  7.7 1.8 pad_maximum_fusion.3
  10.7 2.2 constant_dynamic-slice_fusion.3
  13.0 2.1 constant_dynamic-slice_fusion.2
  16.3 70.8 %all-gather.5.cloned.1.call-done = bf16[2048,1024]{0,1:T(8,128)(2,1)} async-done(((bf16[256,1024]{0,1:T(8,128)(2,1)}), bf16[2048,1024]{0,1:T(8,128)(2,1)}) %all-gather.5.cloned.1.call-update) | async-done | bytes 4194320 | tf_op jit(solution)/shard_map/all_gather | solution.py:185
  87.1 3.7 fusion.41.branch_ref
  90.8 5.6 %mixer.1 = bf16[512,512]{1,0:T(8,128)(2,1)} custom-call(bf16[512,512]{1,0:T(8,128)(2,1)} %fusion.41.branch_ref, f32[4,512]{1,0:T(4,128)} %taps_ref.1, f32[1,512]{1,0:T(1,128)} %bitcast.18, bf16[4,128,128]{2,1,0:T(8,128)(2,1)} %recur_ref.1, f32[1,512]{1,0:T(1,128)} %bitcast.19, bf16[4,128,128]{2,1,0:T(8,128)(2,1)} %input_ref.1, f32[1,512]{1,0:T(1,128)} %bitcast.20, ...), custom_call_target="tpu_custom_call" | custom-call | flops 149946368 | bytes 1048576 | tf_op jit(solution)/shard_map/mixer/pallas_call | solution.py:75
  96.4 4.3 %convolution_convert_fusion.2 = bf16[512,2048]{1,0:T(8,128)(2,1)} fusion(bf16[512,512]{1,0:T(8,128)(2,1)} %mixer.1, bf16[2048,1024]{0,1:T(8,128)(2,1)} %all-gather.5.cloned.1.call-done), kind=kOutput, calls=%fused_computation.68 | convolution fusion | flops 1074790400 | bytes 4718592 | tf_op jit(solution)/shard_map/dot_general | solution.py:206
  100.7 1.3 constant_dynamic-slice_fusion.5
  102.1 48.2 %all-gather.7.cloned.1.call-done = bf16[1024,1536]{1,0:T(8,128)(2,1)} async-done(((bf16[256,1536]{1,0:T(8,128)(2,1)}), bf16[1024,1536]{1,0:T(8,128)(2,1)}) %all-gather.7.cloned.1.call-update) | async-done | bytes 3145744 | tf_op jit(solution)/shard_map/all_gather | solution.py:118
  150.3 1.5 collective-permute-start.2
  151.8 2.2 fusion.27
  154.0 1.3 fusion.29
  155.3 1.5 collective-permute-start.5
  157.8 56.2 %all-gather.9.cloned.1.call-done = bf16[1024,1536]{1,0:T(8,128)(2,1)} async-done(((bf16[256,1536]{1,0:T(8,128)(2,1)}), bf16[1024,1536]{1,0:T(8,128)(2,1)}) %all-gather.9.cloned.1.call-update) | async-done | bytes 3145744 | tf_op jit(solution)/shard_map/all_gather | solution.py:118
  214.0 1.5 collective-permute-start.3
  216.5 2.4 copy-done.17
  218.9 3.4 fusion.50
  222.3 1.8 fusion.51
  224.2 5.4 %fusion.22 = f32[512,1536]{1,0:T(8,128)} fusion(f32[512,1536]{1,0:T(8,128)S(1)} %fusion.51, bf16[1024,1536]{1,0:T(8,128)(2,1)} %collective-permute-done.2, bf16[512,1024]{1,0:T(8,128)(2,1)S(1)} %fusion.47, pred[]{:T(512)S(6)} %eq.5, bf16[512,256]{1,0:T(8,128)(2,1)S(1)} %get-tuple-element.15, bf16[512,256]{1,0:T(8,128)(2,1)S(1)} %get-tuple-element.14, ...), kind=kOutput, calls=%fused_computation.61 | convolution fusion | flops 1617690624 | bytes 11534337 | tf_op jit(solution)/shard_map/dot_general | solution.py:222
  230.2 3.5 fusion.52
  233.8 1.8 fusion.53
  235.6 5.4 %fusion.25 = f32[512,1536]{1,0:T(8,128)} fusion(f32[512,1536]{1,0:T(8,128)S(1)} %fusion.53, bf16[1024,1536]{1,0:T(8,128)(2,1)} %collective-permute-done.2, bf16[512,1024]{1,0:T(8,128)(2,1)S(1)} %fusion.49, pred[]{:T(512)S(6)} %eq.5, bf16[512,256]{1,0:T(8,128)(2,1)S(1)} %get-tuple-element.24, bf16[512,256]{1,0:T(8,128)(2,1)S(1)} %get-tuple-element.23, ...), kind=kOutput, calls=%fused_computation.64 | convolution fusion | flops 1617690624 | bytes 11534337 | tf_op jit(solution)/shard_map/dot_general | solution.py:222
  241.1 83.9 %collective-permute-done.3 = bf16[1024,1536]{1,0:T(8,128)(2,1)} collective-permute-done((bf16[1024,1536]{1,0:T(8,128)(2,1)}, bf16[1024,1536]{1,0:T(8,128)(2,1)}, u32[]{:S(2)}, u32[]{:S(2)}) %collective-permute-start.3) | collective-permute-done | bytes 3145760 | tf_op jit(solution)/shard_map/ppermute | solution.py:119
  325.0 24.1 %all-gather.11.cloned.1.call-done = bf16[1536,2048]{1,0:T(8,128)(2,1)} async-done(((bf16[1536,256]{1,0:T(8,128)(2,1)}), bf16[1536,2048]{1,0:T(8,128)(2,1)}) %all-gather.11.cloned.1.call-update) | async-done | bytes 6291472 | tf_op jit(solution)/shard_map/all_gather | solution.py:190
  349.2 15.0 %convolution_convert_fusion = bf16[512,2048]{1,0:T(8,128)(2,1)S(1)} fusion(bf16[1536,2048]{1,0:T(8,128)(2,1)} %all-gather.11.cloned.1.call-done, f32[512,1536]{1,0:T(8,128)} %fusion.25, f32[512,1536]{1,0:T(8,128)} %fusion.52, bf16[1024,1536]{1,0:T(8,128)(2,1)} %collective-permute-done.3, f32[1536]{0:T(1024)S(1)} %get-tuple-element.7, ...), kind=kOutput, calls=%fused_computation.66 | convolution fusion | flops 4852547584 | bytes 19947520 | tf_op jit(solution)/shard_map/dot_general | solution.py:229
  365.2 15.8 %convolution_convert_fusion.1 = bf16[512,2048]{1,0:T(8,128)(2,1)} fusion(bf16[1536,2048]{1,0:T(8,128)(2,1)} %all-gather.11.cloned.1.call-done, f32[512,1536]{1,0:T(8,128)} %fusion.22, f32[512,1536]{1,0:T(8,128)} %fusion.50, bf16[1024,1536]{1,0:T(8,128)(2,1)} %collective-permute-done.3, f32[1536]{0:T(1024)S(1)} %get-tuple-element.7, ...), kind=kOutput, calls=%fused_computation.67 | convolution fusion | flops 4852547584 | bytes 19947520 | tf_op jit(solution)/shard_map/dot_general | solution.py:229
  381.0 1.3 constant_dynamic-slice_fusion.1
  382.9 1.7 add_convert_fusion
  384.5 1.5 collective-permute-start.8
  386.1 23.7 %collective-permute-done.8 = bf16[256,2048]{1,0:T(8,128)(2,1)S(1)} collective-permute-done((bf16[256,2048]{1,0:T(8,128)(2,1)S(1)}, bf16[256,2048]{1,0:T(8,128)(2,1)S(1)}, u32[]{:S(2)}, u32[]{:S(2)}) %collective-permute-start.8) | collective-permute-done | bytes 1048608 | tf_op jit(solution)/shard_map/ppermute | solution.py:109
  410.6 2.6 collective-permute-done.9
  413.4 1.6 pad_maximum_fusion
  (75 shorter events, 9.0 us)
Async XLA Ops:
  6.5 3.1 copy-start
  6.5 80.5 %all-gather.5.cloned.1.call-start = ((), (), s32[]{:S(2)}) async-start(), calls=%async_computation | async-start | bytes 4718592 | tf_op jit(solution)/shard_map/all_gather | solution.py:185
  9.6 140.7 %all-gather.7.cloned.1.call-start = ((), (), s32[]{:S(2)}) async-start(), calls=%async_computation.1 | async-start | bytes 3932160 | tf_op jit(solution)/shard_map/all_gather | solution.py:118
  10.6 4.5 %copy-start.2 = (bf16[512,2048]{1,0:T(8,128)(2,1)S(1)}, bf16[512,2048]{1,0:T(8,128)(2,1)}, u32[]{:S(2)}) copy-start(bf16[512,2048]{1,0:T(8,128)(2,1)} %param.17) | copy-start | bytes 6291460
  10.6 203.4 %all-gather.9.cloned.1.call-start = ((), (), s32[]{:S(2)}) async-start(), calls=%async_computation.2 | async-start | bytes 3932160 | tf_op jit(solution)/shard_map/all_gather | solution.py:118
  12.9 2.7 copy-start.15
  12.9 74.1 %copy-start.18 = (f32[2048]{0:T(1024)S(1)}, f32[2048]{0:T(1024)}, u32[]{:S(2)}) copy-start(f32[2048]{0:T(1024)} %param.18) | copy-start | bytes 24580
  13.0 336.2 %all-gather.11.cloned.1.call-start = ((), (), s32[]{:S(2)}) async-start(), calls=%async_computation.3 | async-start | bytes 7077888 | tf_op jit(solution)/shard_map/all_gather | solution.py:190
  102.0 49.7 %collective-permute-start = (bf16[256,2048]{1,0:T(8,128)(2,1)S(1)}, bf16[256,2048]{1,0:T(8,128)(2,1)}, u32[]{:S(2)}, u32[]{:S(2)}) collective-permute-start(bf16[256,2048]{1,0:T(8,128)(2,1)S(1)} %constant_dynamic-slice_fusion.5), channel_id=1, source_target_pairs={{0,1},{1,0},{2,3},{3,2},{4,5},{5,4},{6,7},{7,6},{8,9},{9,8},{10,11... | collective-permute-start | bytes 3145736 | tf_op jit(solution)/shard_map/ppermute | solution.py:109
  102.1 51.9 %copy-start.13 = (f32[2048]{0:T(1024)S(1)}, f32[2048]{0:T(1024)}, u32[]{:S(2)}) copy-start(f32[2048]{0:T(1024)} %param.28) | copy-start | bytes 24580
  150.3 73.9 %collective-permute-start.2 = (bf16[1024,1536]{1,0:T(8,128)(2,1)}, bf16[1024,1536]{1,0:T(8,128)(2,1)}, u32[]{:S(2)}, u32[]{:S(2)}) collective-permute-start(bf16[1024,1536]{1,0:T(8,128)(2,1)} %all-gather.7.cloned.1.call-done), channel_id=1, source_target_pairs={{0,2},{2,0},{4,6},{6,4},{8,10},{10,8},{12,14},{14,12},{1,3},{3,1},... | collective-permute-start | bytes 9437192 | tf_op jit(solution)/shard_map/ppermute | solution.py:119
  153.9 2.8 copy-start.14
  155.3 60.2 %collective-permute-start.5 = (bf16[256,2048]{1,0:T(8,128)(2,1)}, bf16[256,2048]{1,0:T(8,128)(2,1)S(1)}, u32[]{:S(2)}, u32[]{:S(2)}) collective-permute-start(bf16[256,2048]{1,0:T(8,128)(2,1)} %fusion.29), channel_id=1, source_target_pairs={{0,16},{16,0},{1,17},{17,1},{2,18},{18,2},{3,19},{19,3},{4,20},{20... | collective-permute-start | bytes 3145736 | tf_op jit(solution)/shard_map/ppermute | solution.py:109
  156.7 58.7 %collective-permute-start.1 = (bf16[256,2048]{1,0:T(8,128)(2,1)}, bf16[256,2048]{1,0:T(8,128)(2,1)S(1)}, u32[]{:S(2)}, u32[]{:S(2)}) collective-permute-start(bf16[256,2048]{1,0:T(8,128)(2,1)} %fusion.29), channel_id=1, source_target_pairs={{0,1},{1,0},{2,3},{3,2},{4,5},{5,4},{6,7},{7,6},{8,9},{9,8},{10,11... | collective-permute-start | bytes 3145736 | tf_op jit(solution)/shard_map/ppermute | solution.py:109
  214.0 111.0 %collective-permute-start.3 = (bf16[1024,1536]{1,0:T(8,128)(2,1)}, bf16[1024,1536]{1,0:T(8,128)(2,1)}, u32[]{:S(2)}, u32[]{:S(2)}) collective-permute-start(bf16[1024,1536]{1,0:T(8,128)(2,1)} %all-gather.9.cloned.1.call-done), channel_id=1, source_target_pairs={{0,2},{2,0},{4,6},{6,4},{8,10},{10,8},{12,14},{14,12},{1,3},{3,1},... | collective-permute-start | bytes 9437192 | tf_op jit(solution)/shard_map/ppermute | solution.py:119
  215.5 14.2 %collective-permute-start.6 = (bf16[256,2048]{1,0:T(8,128)(2,1)S(1)}, bf16[256,2048]{1,0:T(8,128)(2,1)S(1)}, u32[]{:S(2)}, u32[]{:S(2)}) collective-permute-start(bf16[256,2048]{1,0:T(8,128)(2,1)S(1)} %collective-permute-done.5), channel_id=1, source_target_pairs={{0,1},{1,0},{2,3},{3,2},{4,5},{5,4},{6,7},{7,6},{8,9},{9,8},{10,11... | collective-permute-start | bytes 3145736 | tf_op jit(solution)/shard_map/ppermute | solution.py:109
  216.3 7.9 %copy-start.6 = (bf16[512,256]{1,0:T(8,128)(2,1)}, bf16[512,256]{1,0:T(8,128)(2,1)S(1)}, u32[]{:S(2)}) copy-start(bf16[512,256]{1,0:T(8,128)(2,1)S(1)} %get-tuple-element.13) | copy-start | bytes 786436
  216.3 7.9 %copy-start.7 = (bf16[512,256]{1,0:T(8,128)(2,1)}, bf16[512,256]{1,0:T(8,128)(2,1)S(1)}, u32[]{:S(2)}) copy-start(bf16[512,256]{1,0:T(8,128)(2,1)S(1)} %get-tuple-element.14) | copy-start | bytes 786436
  216.3 7.9 %copy-start.8 = (bf16[512,256]{1,0:T(8,128)(2,1)}, bf16[512,256]{1,0:T(8,128)(2,1)S(1)}, u32[]{:S(2)}) copy-start(bf16[512,256]{1,0:T(8,128)(2,1)S(1)} %get-tuple-element.15) | copy-start | bytes 786436
  216.3 2.5 copy-start.17
  216.5 7.7 %copy-start.4 = (bf16[512,1024]{1,0:T(8,128)(2,1)}, bf16[512,1024]{1,0:T(8,128)(2,1)S(1)}, u32[]{:S(2)}) copy-start(bf16[512,1024]{1,0:T(8,128)(2,1)S(1)} %fusion.47) | copy-start | bytes 3145732
  218.9 3.5 copy-start.16
  230.0 5.5 %copy-start.9 = (bf16[512,256]{1,0:T(8,128)(2,1)}, bf16[512,256]{1,0:T(8,128)(2,1)S(1)}, u32[]{:S(2)}) copy-start(bf16[512,256]{1,0:T(8,128)(2,1)S(1)} %get-tuple-element.21) | copy-start | bytes 786436
  230.1 5.5 %copy-start.10 = (bf16[512,256]{1,0:T(8,128)(2,1)}, bf16[512,256]{1,0:T(8,128)(2,1)S(1)}, u32[]{:S(2)}) copy-start(bf16[512,256]{1,0:T(8,128)(2,1)S(1)} %get-tuple-element.22) | copy-start | bytes 786436
  230.1 5.5 %copy-start.11 = (bf16[512,256]{1,0:T(8,128)(2,1)}, bf16[512,256]{1,0:T(8,128)(2,1)S(1)}, u32[]{:S(2)}) copy-start(bf16[512,256]{1,0:T(8,128)(2,1)S(1)} %get-tuple-element.23) | copy-start | bytes 786436
  230.1 5.5 %copy-start.12 = (bf16[512,256]{1,0:T(8,128)(2,1)}, bf16[512,256]{1,0:T(8,128)(2,1)S(1)}, u32[]{:S(2)}) copy-start(bf16[512,256]{1,0:T(8,128)(2,1)S(1)} %get-tuple-element.24) | copy-start | bytes 786436
  230.2 5.4 %copy-start.5 = (bf16[512,1024]{1,0:T(8,128)(2,1)}, bf16[512,1024]{1,0:T(8,128)(2,1)S(1)}, u32[]{:S(2)}) copy-start(bf16[512,1024]{1,0:T(8,128)(2,1)S(1)} %fusion.49) | copy-start | bytes 3145732
  365.2 17.7 %collective-permute-start.7 = (bf16[256,2048]{1,0:T(8,128)(2,1)}, bf16[256,2048]{1,0:T(8,128)(2,1)}, u32[]{:S(2)}, u32[]{:S(2)}) collective-permute-start(bf16[256,2048]{1,0:T(8,128)(2,1)} %constant_dynamic-slice_fusion), channel_id=1, source_target_pairs={{0,1},{1,0},{2,3},{3,2},{4,5},{5,4},{6,7},{7,6},{8,9},{9,8},{10,11... | collective-permute-start | bytes 3145736 | tf_op jit(solution)/shard_map/ppermute | solution.py:109
  382.3 27.5 %copy-start.3 = (bf16[512,2048]{1,0:T(8,128)(2,1)S(1)}, bf16[512,2048]{1,0:T(8,128)(2,1)}, u32[]{:S(2)}) copy-start(bf16[512,2048]{1,0:T(8,128)(2,1)} %convolution_convert_fusion.1) | copy-start | bytes 6291460
  382.3 3.8 collective-permute-start.4
  384.5 25.2 %collective-permute-start.8 = (bf16[256,2048]{1,0:T(8,128)(2,1)S(1)}, bf16[256,2048]{1,0:T(8,128)(2,1)S(1)}, u32[]{:S(2)}, u32[]{:S(2)}) collective-permute-start(bf16[256,2048]{1,0:T(8,128)(2,1)S(1)} %add_convert_fusion), channel_id=1, source_target_pairs={{0,16},{16,0},{1,17},{17,1},{2,18},{18,2},{3,19},{19,3},{4,20},{20... | collective-permute-start | bytes 3145736 | tf_op jit(solution)/shard_map/ppermute | solution.py:109
  410.5 2.7 collective-permute-start.9
  (1 other events, 1.9 us)
Sparse Core Ops, SparseCore 0:
  9.7 77.3 all-gather.4
  88.6 61.6 all-gather.6
  151.9 62.0 all-gather.8
  215.9 133.2 all-gather.10
